TPU v7x, 32 devices: a whole 2x2x4 slice. The times are simulated.
32 devices in a mesh: fs: 8 (over z, x), tp: 4 (over y, core).
Axes of the slice: x: 2, y: 2, z: 4, core: 2. Of those that a mesh axis runs over, the one named last changes fastest.
Arguments:
- normed_input: bfloat16 [16384, 2048], P('fs'), may hold values from -6 to 6
- gate_cotangent: bfloat16 [16384, 2048], P('fs', 'tp'), may hold values from -0.125 to 0.125
- first_value_cot: bfloat16 [16384, 1024], P('fs', 'tp'), may hold values from -0.125 to 0.125
- second_value_cot: bfloat16 [16384, 1024], P('fs', 'tp'), may hold values from -0.125 to 0.125
- head_lambda: float32 [8], P('tp'), may hold values from 0.3 to 0.8
- projection: bfloat16 [2048, 256], replicated, may hold values from -1 to 1, as said below
- gate_weight: float32 [2048, 2048], P('fs', 'tp'), may hold values from -0.125 to 0.125
- gate_first: float32 [256, 2048], P('fs', 'tp'), may hold values from -1.5 to 1.5
- gate_second: float32 [256, 2048], P('fs', 'tp'), may hold values from 0.01 to 1
- value_weight: float32 [2048, 1024], P('fs', 'tp'), may hold values from -0.125 to 0.125
- value_first: float32 [256, 1024], P('fs', 'tp'), may hold values from -1.5 to 1.5
- value_second: float32 [256, 1024], P('fs', 'tp'), may hold values from 0.01 to 1
Outputs:
- new_gate_weight: float32 [2048, 2048], P('fs', 'tp')
- gate_step: float32 [2048, 2048], P('fs', 'tp')
- gate_copy: bfloat16 [2048, 2048], P(None, 'tp')
- new_gate_first: float32 [256, 2048], P('fs', 'tp')
- new_gate_second: float32 [256, 2048], P('fs', 'tp')
- new_value_weight: float32 [2048, 1024], P('fs', 'tp')
- value_step: float32 [2048, 1024], P('fs', 'tp')
- value_copy: bfloat16 [2048, 1024], P(None, 'tp')
- new_value_first: float32 [256, 1024], P('fs', 'tp')
- new_value_second: float32 [256, 1024], P('fs', 'tp')
Inputs may be any that keep to these rules, and one draw needn't show every extreme that they name: `projection`: a low-rank factor whose rows differ in scale.
All inputs are finite; a program needn't handle non-finite values.
Results may differ from a plain program's by a relative error of at most 0.0054.
Values may be sent and summed in bfloat16 or wider, within the bound.
No kernel may reach another device: no remote copies, remote signals or barrier semaphores. Data moves between devices by JAX's collectives and lax.ppermute only.
A program may use at most 64 MiB of HBM per device.

v0:
```python
import jax
import jax.numpy as jnp
from jax import lax
from jax.sharding import PartitionSpec as P

D = 2048
HEADS = 8
VDIM = 128
moment_decay = 0.9
square_decay = 0.95
adam_floor = 1e-08
learn_rate = 0.02
rms_floor = 0.1


def across_tokens(left, right, precision=None):
    return lax.dot_general(
        left,
        right,
        (((0,), (0,)), ((), ())),
        preferred_element_type=jnp.float32,
        precision=precision,
    )


def moments(first, second, low):
    new_first = moment_decay * first + (1.0 - moment_decay) * low
    new_second = square_decay * second + (1.0 - square_decay) * low * low
    return (new_first, new_second, new_first / (jnp.sqrt(new_second) + adam_floor))


def split_product(stacked, cotangent, factors):
    both = across_tokens(stacked, cotangent)
    return both[:factors] + both[factors:]


def per_device(
    normed_input,
    gate_cotangent,
    first_value_cot,
    second_value_cot,
    head_lambda,
    projection,
    gate_weight,
    gate_first,
    gate_second,
    value_weight,
    value_first,
    value_second,
):
    highest = lax.Precision.HIGHEST
    column_lambda = jnp.repeat(head_lambda, VDIM)
    value_cot = (
        first_value_cot.astype(jnp.float32)
        - column_lambda[None, :] * second_value_cot.astype(jnp.float32)
    ).astype(jnp.bfloat16)
    rows_here = gate_weight.shape[0]
    first_row = lax.axis_index("fs") * rows_here
    local_factor = lax.dynamic_slice_in_dim(projection, first_row, rows_here, 0).astype(jnp.float32)
    projected = jnp.dot(normed_input, projection, preferred_element_type=jnp.float32)
    upper = projected.astype(jnp.bfloat16)
    upper_wide = lax.optimization_barrier(upper).astype(jnp.float32)
    lower = (projected - upper_wide).astype(jnp.bfloat16)
    stacked = jnp.concatenate([upper, lower], axis=1)
    factors = projection.shape[1]
    partial_gate = split_product(stacked, gate_cotangent, factors)
    partial_value = split_product(stacked, value_cot, factors)
    gate_low, value_low = (
        lax.psum_scatter(partial_gate, "fs", scatter_dimension=0, tiled=True),
        lax.psum_scatter(partial_value, "fs", scatter_dimension=0, tiled=True),
    )
    new_gate_first, new_gate_second, gate_dir = moments(gate_first, gate_second, gate_low)
    new_value_first, new_value_second, value_dir = moments(value_first, value_second, value_low)
    gate_update = jnp.dot(
        local_factor, lax.all_gather(gate_dir, "fs", axis=0, tiled=True), precision=highest
    )
    value_update = jnp.dot(
        local_factor, lax.all_gather(value_dir, "fs", axis=0, tiled=True), precision=highest
    )
    gate_total, value_total = lax.psum(
        (jnp.sum(gate_update * gate_update), jnp.sum(value_update * value_update)), ("fs", "tp")
    )
    gate_step = gate_update / (jnp.sqrt(gate_total / (D * D)) + rms_floor)
    value_step = value_update / (jnp.sqrt(value_total / (D * HEADS * VDIM)) + rms_floor)
    new_gate_weight = gate_weight - learn_rate * gate_step
    new_value_weight = value_weight - learn_rate * value_step
    gate_copy, value_copy = (
        lax.all_gather(new_gate_weight.astype(jnp.bfloat16), "fs", axis=0, tiled=True),
        lax.all_gather(new_value_weight.astype(jnp.bfloat16), "fs", axis=0, tiled=True),
    )
    return (
        new_gate_weight,
        gate_step,
        gate_copy,
        new_gate_first,
        new_gate_second,
        new_value_weight,
        value_step,
        value_copy,
        new_value_first,
        new_value_second,
    )


def solution(mesh):
    placed = (
        P("fs", None),
        P("fs", "tp"),
        P("fs", "tp"),
        P("fs", "tp"),
        P("tp"),
        P(),
        P("fs", "tp"),
        P("fs", "tp"),
        P("fs", "tp"),
        P("fs", "tp"),
        P("fs", "tp"),
        P("fs", "tp"),
    )
    return jax.shard_map(
        per_device,
        mesh=mesh,
        in_specs=placed,
        out_specs=(
            P("fs", "tp"),
            P("fs", "tp"),
            P(None, "tp"),
            P("fs", "tp"),
            P("fs", "tp"),
            P("fs", "tp"),
            P("fs", "tp"),
            P(None, "tp"),
            P("fs", "tp"),
            P("fs", "tp"),
        ),
        check_vma=False,
    )
```

profile of v0, /device:TPU:0, one launch (start us, length us, event | category | flops | bytes accessed | tf_op | source)
XLA Modules:
  0.0 325.0 jit_solution(1942997298936797233)
XLA Ops:
  7.2 6.1 %fusion.17 = (bf16[2048,256]{0,1:T(8,128)(2,1)S(1)}, f32[2048,256]{0,1:T(8,128)S(1)}) fusion(bf16[2048,2048]{1,0:T(8,128)(2,1)} %param.12, bf16[2048,256]{1,0:T(8,128)(2,1)} %param.17), kind=kOutput, calls=%fused_computation.33 | convolution fusion | flops 2148007936 | bytes 12582912 | tf_op jit(solution)/shard_map/dot_general | solution.py:60
  13.5 0.3 subtract_convert_fusion.1
  13.7 0.9 copy-done.8
  14.7 0.3 copy-done.9
  15.0 0.8 fusion
  15.8 0.2 copy-done.2
  16.0 0.7 slice_add_fusion.1
  16.8 2.5 fusion.1
  19.3 0.9 slice_add_fusion
  20.3 61.4 %reduce-scatter.5.cloned.1.call-done = f32[32,256]{1,0:T(8,128)} async-done(((f32[256,256]{1,0:T(8,128)}), f32[32,256]{1,0:T(8,128)}) %reduce-scatter.5.cloned.1.call-update) | async-done | bytes 32784 | tf_op jit(solution)/shard_map/reduce_scatter | solution.py:70
  81.7 1.4 add_divide_fusion.1
  83.1 31.1 %all_gather.14 = f32[256,256]{1,0:T(8,128)S(1)} all-gather(f32[32,256]{1,0:T(8,128)S(1)} %get-tuple-element.18), channel_id=1, replica_groups=mesh['fs'=8,'tp'=4] {'fs'}, dimensions={0}, use_global_device_ids=true | all-gather | bytes 294912 | tf_op jit(solution)/shard_map/all_gather | solution.py:78
  114.2 1.9 multiply_reduce_fusion.1
  116.1 31.3 %reduce-scatter.3.cloned.1.call-done = f32[32,512]{1,0:T(8,128)} async-done(((f32[256,512]{1,0:T(8,128)}), f32[32,512]{1,0:T(8,128)}) %reduce-scatter.3.cloned.1.call-update) | async-done | bytes 65552 | tf_op jit(solution)/shard_map/reduce_scatter | solution.py:69
  147.4 1.5 add_divide_fusion
  148.9 31.4 %all_gather.12 = f32[256,512]{1,0:T(8,128)S(1)} all-gather(f32[32,512]{1,0:T(8,128)S(1)} %get-tuple-element.21), channel_id=1, replica_groups=mesh['fs'=8,'tp'=4] {'fs'}, dimensions={0}, use_global_device_ids=true | all-gather | bytes 589824 | tf_op jit(solution)/shard_map/all_gather | solution.py:75
  180.4 2.0 multiply_reduce_fusion
  182.4 37.8 %all-reduce = (f32[]{:T(128)}, f32[]{:T(128)}) all-reduce(f32[]{:T(128)} %get-tuple-element.26, f32[]{:T(128)} %get-tuple-element.28), channel_id=1, replica_groups=mesh['fs'=8,'tp'=4] {'fs','tp'}, use_global_device_ids=true, to_apply=%region_2.0 | all-reduce | flops 2 | bytes 16 | tf_op jit(solution)/shard_map/psum | solution.py:80
  220.8 1.8 fusion.13
  223.4 1.2 fusion.14
  224.7 39.3 %all-gather.5.cloned.1.call-done = bf16[2048,256]{1,0:T(8,128)(2,1)} async-done(((bf16[256,256]{1,0:T(8,128)(2,1)}), bf16[2048,256]{1,0:T(8,128)(2,1)}) %all-gather.5.cloned.1.call-update) | async-done | bytes 1048592 | tf_op jit(solution)/shard_map/all_gather | solution.py:89
  263.9 50.4 %all-gather.3.cloned.1.call-done = bf16[2048,512]{1,0:T(8,128)(2,1)} async-done(((bf16[256,512]{1,0:T(8,128)(2,1)}), bf16[2048,512]{1,0:T(8,128)(2,1)}) %all-gather.3.cloned.1.call-update) | async-done | bytes 2097168 | tf_op jit(solution)/shard_map/all_gather | solution.py:88
  314.3 3.1 copy.24
  317.5 1.0 copy.25
  (28 shorter events, 0.3 us)
Async XLA Ops:
  7.2 9.6 %copy-start = (bf16[2048,512]{1,0:T(8,128)(2,1)S(1)}, bf16[2048,512]{1,0:T(8,128)(2,1)}, u32[]{:S(2)}) copy-start(bf16[2048,512]{1,0:T(8,128)(2,1)} %param.13) | copy-start | bytes 6291460
  7.2 6.2 %copy-start.10 = (f32[2]{0:T(128)S(1)}, f32[2]{0:T(128)}, u32[]{:S(2)}) copy-start(f32[2]{0:T(128)} %param.16) | copy-start | bytes 28
  7.2 74.5 %reduce-scatter.5.cloned.1.call-start = ((), (), s32[]{:S(2)}) async-start(), calls=%async_computation.4 | async-start | bytes 294912 | tf_op jit(solution)/shard_map/reduce_scatter | solution.py:70
  13.5 1.2 copy-start.8
  13.5 1.5 copy-start.9
  15.0 1.0 copy-start.2
  16.7 130.7 %reduce-scatter.3.cloned.1.call-start = ((), (), s32[]{:S(2)}) async-start(), calls=%async_computation.2 | async-start | bytes 589824 | tf_op jit(solution)/shard_map/reduce_scatter | solution.py:69
  19.3 62.4 %copy-start.6 = (f32[32,256]{1,0:T(8,128)S(1)}, f32[32,256]{1,0:T(8,128)}, u32[]{:S(2)}) copy-start(f32[32,256]{1,0:T(8,128)} %param.23) | copy-start | bytes 98308
  19.3 62.4 %copy-start.7 = (f32[32,256]{1,0:T(8,128)S(1)}, f32[32,256]{1,0:T(8,128)}, u32[]{:S(2)}) copy-start(f32[32,256]{1,0:T(8,128)} %param.22) | copy-start | bytes 98308
  19.3 128.1 %copy-start.4 = (f32[32,512]{1,0:T(8,128)S(1)}, f32[32,512]{1,0:T(8,128)}, u32[]{:S(2)}) copy-start(f32[32,512]{1,0:T(8,128)} %param.20) | copy-start | bytes 196612
  19.3 128.1 %copy-start.5 = (f32[32,512]{1,0:T(8,128)S(1)}, f32[32,512]{1,0:T(8,128)}, u32[]{:S(2)}) copy-start(f32[32,512]{1,0:T(8,128)} %param.19) | copy-start | bytes 196612
  20.2 243.7 %all-gather.5.cloned.1.call-start = ((), (), s32[]{:S(2)}) async-start(), calls=%async_computation.5 | async-start | bytes 1179648 | tf_op jit(solution)/shard_map/all_gather | solution.py:89
  114.2 109.2 %copy-start.3 = (f32[256,512]{1,0:T(8,128)S(1)}, f32[256,512]{1,0:T(8,128)}, u32[]{:S(2)}) copy-start(f32[256,512]{1,0:T(8,128)} %param.18) | copy-start | bytes 1572868
  222.7 91.6 %all-gather.3.cloned.1.call-start = ((), (), s32[]{:S(2)}) async-start(), calls=%async_computation.3 | async-start | bytes 2359296 | tf_op jit(solution)/shard_map/all_gather | solution.py:88
  314.3 3.1 copy-start.1
Sparse Core Ops, SparseCore 0:
  16.8 64.8 reduce-scatter.4
  85.6 61.7 reduce-scatter.2
  222.8 41.0 all-gather.4
  266.5 47.7 all-gather.2
where the time goes:
time: 325 us
  waiting for transfers between devices  182 us (56%)
  blocking collectives  100 us (31%)
  between operations  15.3 us (5%)
  matrix products  13.3 us (4%)
  other arithmetic  7.83 us (2%)
  local copies, waits for them, and re-layouts  5.67 us (2%)
    reduce_scatter x1, waiting for transfers between devices, per_device(): lax.psum_scatter(partial_value, 'fs', scatter_dimension=0, tiled=True)  61.4 us
    all_gather x1, waiting for transfers between devices, per_device(): lax.all_gather(new_gate_weight.astype(jnp.bfloat16), 'fs', axis=0, tiled=...  50.4 us
    all_gather x1, waiting for transfers between devices, per_device(): lax.all_gather(new_value_weight.astype(jnp.bfloat16), 'fs', axis=0, tiled...  39.3 us
    psum x1, blocking collectives, per_device(): lax.psum((jnp.sum(gate_update * gate_update), jnp.sum(value_update * valu...  37.8 us
    all_gather x1, blocking collectives, per_device(): lax.all_gather(gate_dir, 'fs', axis=0, tiled=True)  31.4 us
    reduce_scatter x1, waiting for transfers between devices, per_device(): lax.psum_scatter(partial_gate, 'fs', scatter_dimension=0, tiled=True)  31.3 us
    all_gather x1, blocking collectives, per_device(): lax.all_gather(value_dir, 'fs', axis=0, tiled=True)  31.1 us
  transfers between devices with their start and end apart: 4, of which 4 were waited for; matrix products, arithmetic and copies ran while one was open for 2% of the time, Pallas kernels for 0%

commit v1 on v0

--- a/solution.py
+++ b/solution.py
@@ -78,7 +78,8 @@
         local_factor, lax.all_gather(value_dir, "fs", axis=0, tiled=True), precision=highest
     )
     gate_total, value_total = lax.psum(
-        (jnp.sum(gate_update * gate_update), jnp.sum(value_update * value_update)), ("fs", "tp")
+        lax.psum((jnp.sum(gate_update * gate_update), jnp.sum(value_update * value_update)), "tp"),
+        "fs",
     )
     gate_step = gate_update / (jnp.sqrt(gate_total / (D * D)) + rms_floor)
     value_step = value_update / (jnp.sqrt(value_total / (D * HEADS * VDIM)) + rms_floor)

time: 325 us -> 310 us (0.954)
  blocking collectives: 100 us -> 88.9 us
    psum x1, blocking collectives: 37.8 us -> 6.27 us  [per_device(): lax.psum((jnp.sum(gate_update * gate_update), jnp.sum(value_update * valu...]
    psum x0 -> x1, blocking collectives: none -> 20.1 us  [per_device(): lax.psum(lax.psum((jnp.sum(gate_update * gate_update), jnp.sum(value_upda...]
    all_gather x1, waiting for transfers between devices: 39.3 us -> 35.6 us  [per_device(): lax.all_gather(new_value_weight.astype(jnp.bfloat16), 'fs', axis=0, tiled...]
  transfers between devices with their start and end apart: 4 -> 4, of which waited for: 4 -> 4; matrix products, arithmetic and copies ran while one was open for 2% -> 3% of each run, Pallas kernels for 0% -> 0%
where the time goes in v1:
time: 310 us
  waiting for transfers between devices  179 us (58%)
  blocking collectives  88.9 us (29%)
  between operations  15.3 us (5%)
  matrix products  13.3 us (4%)
  other arithmetic  7.83 us (3%)
  local copies, waits for them, and re-layouts  5.67 us (2%)
    reduce_scatter x1, waiting for transfers between devices, per_device(): lax.psum_scatter(partial_value, 'fs', scatter_dimension=0, tiled=True)  61.4 us
    all_gather x1, waiting for transfers between devices, per_device(): lax.all_gather(new_gate_weight.astype(jnp.bfloat16), 'fs', axis=0, tiled=...  50.4 us
    all_gather x1, waiting for transfers between devices, per_device(): lax.all_gather(new_value_weight.astype(jnp.bfloat16), 'fs', axis=0, tiled...  35.6 us
    all_gather x1, blocking collectives, per_device(): lax.all_gather(gate_dir, 'fs', axis=0, tiled=True)  31.4 us
    reduce_scatter x1, waiting for transfers between devices, per_device(): lax.psum_scatter(partial_gate, 'fs', scatter_dimension=0, tiled=True)  31.3 us
    all_gather x1, blocking collectives, per_device(): lax.all_gather(value_dir, 'fs', axis=0, tiled=True)  31.1 us
    psum x1, blocking collectives, per_device(): lax.psum(lax.psum((jnp.sum(gate_update * gate_update), jnp.sum(value_upda...  20.1 us
    psum x1, blocking collectives, per_device(): lax.psum((jnp.sum(gate_update * gate_update), jnp.sum(value_update * valu...  6.27 us
  transfers between devices with their start and end apart: 4, of which 4 were waited for; matrix products, arithmetic and copies ran while one was open for 3% of the time, Pallas kernels for 0%

profile of v1, /device:TPU:0, one launch (start us, length us, event | category | flops | bytes accessed | tf_op | source)
XLA Modules:
  0.0 309.9 jit_solution(10907425682175702677)
XLA Ops:
  7.2 6.1 %fusion.17 = (bf16[2048,256]{0,1:T(8,128)(2,1)S(1)}, f32[2048,256]{0,1:T(8,128)S(1)}) fusion(bf16[2048,2048]{1,0:T(8,128)(2,1)} %param.12, bf16[2048,256]{1,0:T(8,128)(2,1)} %param.17), kind=kOutput, calls=%fused_computation.33 | convolution fusion | flops 2148007936 | bytes 12582912 | tf_op jit(solution)/shard_map/dot_general | solution.py:60
  13.5 0.3 subtract_convert_fusion.1
  13.7 0.9 copy-done.8
  14.7 0.3 copy-done.9
  15.0 0.8 fusion
  16.0 0.7 slice_add_fusion.1
  16.8 2.5 fusion.1
  19.3 0.9 slice_add_fusion
  20.3 61.4 %reduce-scatter.5.cloned.1.call-done = f32[32,256]{1,0:T(8,128)} async-done(((f32[256,256]{1,0:T(8,128)}), f32[32,256]{1,0:T(8,128)}) %reduce-scatter.5.cloned.1.call-update) | async-done | bytes 32784 | tf_op jit(solution)/shard_map/reduce_scatter | solution.py:70
  81.7 1.4 add_divide_fusion.1
  83.1 31.1 %all_gather.14 = f32[256,256]{1,0:T(8,128)S(1)} all-gather(f32[32,256]{1,0:T(8,128)S(1)} %get-tuple-element.20), channel_id=1, replica_groups=mesh['fs'=8,'tp'=4] {'fs'}, dimensions={0}, use_global_device_ids=true | all-gather | bytes 294912 | tf_op jit(solution)/shard_map/all_gather | solution.py:78
  114.2 1.9 multiply_reduce_fusion.1
  116.1 31.3 %reduce-scatter.3.cloned.1.call-done = f32[32,512]{1,0:T(8,128)} async-done(((f32[256,512]{1,0:T(8,128)}), f32[32,512]{1,0:T(8,128)}) %reduce-scatter.3.cloned.1.call-update) | async-done | bytes 65552 | tf_op jit(solution)/shard_map/reduce_scatter | solution.py:69
  147.4 1.5 add_divide_fusion
  148.9 31.4 %all_gather.12 = f32[256,512]{1,0:T(8,128)S(1)} all-gather(f32[32,512]{1,0:T(8,128)S(1)} %get-tuple-element.23), channel_id=1, replica_groups=mesh['fs'=8,'tp'=4] {'fs'}, dimensions={0}, use_global_device_ids=true | all-gather | bytes 589824 | tf_op jit(solution)/shard_map/all_gather | solution.py:75
  180.4 2.0 multiply_reduce_fusion
  182.4 6.3 %all-reduce.1 = (f32[]{:T(128)}, f32[]{:T(128)}) all-reduce(f32[]{:T(128)} %get-tuple-element.28, f32[]{:T(128)} %get-tuple-element.30), channel_id=1, replica_groups=mesh['fs'=8,'tp'=4] {'tp'}, use_global_device_ids=true, to_apply=%region_2.0 | all-reduce | flops 2 | bytes 16 | tf_op jit(solution)/shard_map/psum | solution.py:81
  188.7 20.1 %all-reduce = (f32[]{:T(128)}, f32[]{:T(128)}) all-reduce(f32[]{:T(128)} %get-tuple-element.12, f32[]{:T(128)} %get-tuple-element.13), channel_id=1, replica_groups=mesh['fs'=8,'tp'=4] {'fs'}, use_global_device_ids=true, to_apply=%region_3.0 | all-reduce | flops 2 | bytes 16 | tf_op jit(solution)/shard_map/psum | solution.py:80
  209.4 1.8 fusion.13
  212.0 1.2 fusion.14
  213.3 35.6 %all-gather.5.cloned.1.call-done = bf16[2048,256]{1,0:T(8,128)(2,1)} async-done(((bf16[256,256]{1,0:T(8,128)(2,1)}), bf16[2048,256]{1,0:T(8,128)(2,1)}) %all-gather.5.cloned.1.call-update) | async-done | bytes 1048592 | tf_op jit(solution)/shard_map/all_gather | solution.py:90
  248.8 50.4 %all-gather.3.cloned.1.call-done = bf16[2048,512]{1,0:T(8,128)(2,1)} async-done(((bf16[256,512]{1,0:T(8,128)(2,1)}), bf16[2048,512]{1,0:T(8,128)(2,1)}) %all-gather.3.cloned.1.call-update) | async-done | bytes 2097168 | tf_op jit(solution)/shard_map/all_gather | solution.py:89
  299.2 3.1 %copy.24 = bf16[2048,512]{1,0:T(8,128)(2,1)} copy(bf16[2048,512]{1,0:T(8,128)(2,1)} %all-gather.3.cloned.1.call-done) | data formatting | bytes 4194304
  302.4 1.0 copy.25
  (29 shorter events, 0.5 us)
Async XLA Ops:
  7.2 9.6 %copy-start = (bf16[2048,512]{1,0:T(8,128)(2,1)S(1)}, bf16[2048,512]{1,0:T(8,128)(2,1)}, u32[]{:S(2)}) copy-start(bf16[2048,512]{1,0:T(8,128)(2,1)} %param.13) | copy-start | bytes 6291460
  7.2 6.2 %copy-start.10 = (f32[2]{0:T(128)S(1)}, f32[2]{0:T(128)}, u32[]{:S(2)}) copy-start(f32[2]{0:T(128)} %param.16) | copy-start | bytes 28
  7.2 74.5 %reduce-scatter.5.cloned.1.call-start = ((), (), s32[]{:S(2)}) async-start(), calls=%async_computation.4 | async-start | bytes 294912 | tf_op jit(solution)/shard_map/reduce_scatter | solution.py:70
  13.5 1.2 copy-start.8
  13.5 1.5 copy-start.9
  15.0 1.0 copy-start.2
  16.7 130.7 %reduce-scatter.3.cloned.1.call-start = ((), (), s32[]{:S(2)}) async-start(), calls=%async_computation.2 | async-start | bytes 589824 | tf_op jit(solution)/shard_map/reduce_scatter | solution.py:69
  19.3 62.4 %copy-start.6 = (f32[32,256]{1,0:T(8,128)S(1)}, f32[32,256]{1,0:T(8,128)}, u32[]{:S(2)}) copy-start(f32[32,256]{1,0:T(8,128)} %param.23) | copy-start | bytes 98308
  19.3 62.4 %copy-start.7 = (f32[32,256]{1,0:T(8,128)S(1)}, f32[32,256]{1,0:T(8,128)}, u32[]{:S(2)}) copy-start(f32[32,256]{1,0:T(8,128)} %param.22) | copy-start | bytes 98308
  19.3 128.1 %copy-start.4 = (f32[32,512]{1,0:T(8,128)S(1)}, f32[32,512]{1,0:T(8,128)}, u32[]{:S(2)}) copy-start(f32[32,512]{1,0:T(8,128)} %param.20) | copy-start | bytes 196612
  19.3 128.1 %copy-start.5 = (f32[32,512]{1,0:T(8,128)S(1)}, f32[32,512]{1,0:T(8,128)}, u32[]{:S(2)}) copy-start(f32[32,512]{1,0:T(8,128)} %param.19) | copy-start | bytes 196612
  20.2 228.6 %all-gather.5.cloned.1.call-start = ((), (), s32[]{:S(2)}) async-start(), calls=%async_computation.5 | async-start | bytes 1179648 | tf_op jit(solution)/shard_map/all_gather | solution.py:90
  114.2 97.8 %copy-start.3 = (f32[256,512]{1,0:T(8,128)S(1)}, f32[256,512]{1,0:T(8,128)}, u32[]{:S(2)}) copy-start(f32[256,512]{1,0:T(8,128)} %param.18) | copy-start | bytes 1572868
  211.3 87.9 %all-gather.3.cloned.1.call-start = ((), (), s32[]{:S(2)}) async-start(), calls=%async_computation.3 | async-start | bytes 2359296 | tf_op jit(solution)/shard_map/all_gather | solution.py:89
  299.2 3.1 %copy-start.1 = (bf16[2048,256]{1,0:T(8,128)(2,1)S(1)}, bf16[2048,256]{1,0:T(8,128)(2,1)}, u32[]{:S(2)}) copy-start(bf16[2048,256]{1,0:T(8,128)(2,1)} %all-gather.5.cloned.1.call-done) | copy-start | bytes 3145732
Sparse Core Ops, SparseCore 0:
  16.8 64.8 reduce-scatter.4
  85.6 61.7 reduce-scatter.2
  211.4 37.3 all-gather.4
  251.4 47.7 all-gather.2
